TPU v7x, 32 devices: a whole 2x2x4 slice. The times are simulated.
32 devices in a mesh: ep: 8 (over z, y), tp: 4 (over x, core).
Axes of the slice: x: 2, y: 2, z: 4, core: 2. Of those that a mesh axis runs over, the one named last changes fastest.
Arguments:
- query: bfloat16 [1024, 1536], P('ep', 'tp'), may hold values from -136 to 136
- latent: bfloat16 [1024, 512], P(('ep', 'tp')), may hold values from -6 to 6
- rope_key: bfloat16 [1024, 32], P(('ep', 'tp')), may hold values from -6 to 6
- latent_gain: float32 [512], replicated, may hold values from 0.1 to 1.9
- key_up: bfloat16 [512, 1024], P(None, 'tp'), may hold values from -0.25 to 0.25
- value_up: bfloat16 [512, 1024], P(None, 'tp'), may hold values from -2 to 2
- out_proj: bfloat16 [1024, 2048], replicated, may hold values from -0.1875 to 0.1875
- tokens: bfloat16 [2048, 2048], P(('ep', 'tp')), may hold values from -6 to 6
- moe_gain: float32 [2048], replicated, may hold values from 0.1 to 1.9
- routes: int32 [2048, 2], P(('ep', 'tp')), may hold values from 0 to 7, all different within a row; in each aligned block of 64 rows (0 to 63, 64 to 127, ...) at most 32 rows name the same one
- group_prob: float32 [2048], P(('ep', 'tp')), may hold values from 0.25 to 1
- expert_prob: float32 [2048, 2], P(('ep', 'tp')), may hold values from 0.02 to 1
- w_gate: bfloat16 [8, 2048, 1024], P('ep', None, 'tp'), may hold values from -0.125 to 0.125
- w_up: bfloat16 [8, 2048, 1024], P('ep', None, 'tp'), may hold values from -0.125 to 0.125
- w_down: bfloat16 [8, 1024, 2048], P('ep', 'tp'), may hold values from -0.1875 to 0.1875
Outputs:
- mixed: bfloat16 [1024, 2048], P(('ep', 'tp'))
- moe_out: bfloat16 [2048, 2048], P(('ep', 'tp'))
Inputs may be any that keep to these rules, and one draw needn't show every extreme that they name: `routes`: each row names 2 different experts; within the rows of one device no expert is named more than 32 times.
All inputs are finite; a program needn't handle non-finite values.
Results may differ from a plain program's by a relative error of at most 0.025.
Values may be sent and summed in bfloat16 or wider, within the bound.
A program may use at most 128 MiB of HBM per device.

v0:
```python
import math
import jax
import jax.numpy as jnp
from jax import lax
from jax.sharding import PartitionSpec as P

NOPE = 64
ROPE_DIM = 32
V_DIM = 64
epsilon = 1e-06
rope_base = 10000.0
masked_value = -1e30


def rms_scale(values, gain):
    widened = values.astype(jnp.float32)
    return widened * lax.rsqrt(jnp.mean(widened * widened, axis=-1, keepdims=True) + epsilon) * gain


def tables(positions, rope_width):
    half_width = rope_width // 2
    inverse = rope_base ** (-2.0 * jnp.arange(half_width, dtype=jnp.float32) / rope_width)
    angles = positions.astype(jnp.float32)[:, None] * inverse[None, :]
    return (jnp.cos(angles), jnp.sin(angles))


def rotate(values, cosine, sine):
    half_width = values.shape[-1] // 2
    lower = values[..., :half_width]
    upper = values[..., half_width:]
    return jnp.concatenate([lower * cosine - upper * sine, lower * sine + upper * cosine], axis=-1)


def keep_state(state_in):
    return state_in


def attend_block(running, query_rot, query_pos, key_part, value_part, rope_part):
    amount = key_part.shape[0]
    span_rows = math.gcd(amount, 1024)
    head_count = query_rot.shape[1]
    scale_factor = query_rot.shape[2] ** (-0.5)
    last_query = query_pos[-1]

    def update(state, block_at):
        row_begin = block_at * span_rows
        keys_here = lax.dynamic_slice_in_dim(key_part, row_begin, span_rows, 0).reshape(
            span_rows, head_count, -1
        )
        values_here = lax.dynamic_slice_in_dim(value_part, row_begin, span_rows, 0).reshape(
            span_rows, head_count, -1
        )
        rope_here = lax.dynamic_slice_in_dim(rope_part, row_begin, span_rows, 0)
        key_pos = row_begin + jnp.arange(span_rows, dtype=jnp.int32)

        def advance(state_in):
            top_old, totals, weighted = state_in
            shared = jnp.broadcast_to(
                rope_here[:, None, :], (span_rows, head_count, rope_here.shape[1])
            )
            full_keys = jnp.concatenate([keys_here, shared], axis=-1)
            scores = (
                jnp.einsum("qhd,khd->hqk", query_rot, full_keys, preferred_element_type=jnp.float32)
                * scale_factor
            )
            allowed = key_pos[None, :] <= query_pos[:, None]
            scores = jnp.where(allowed[None], scores, masked_value)
            top_new = jnp.maximum(top_old, jnp.max(scores, axis=-1))
            raised = jnp.where(allowed[None], jnp.exp(scores - top_new[..., None]), 0.0)
            factor = jnp.exp(top_old - top_new)
            totals = totals * factor + jnp.sum(raised, axis=-1)
            weighted = weighted * factor[..., None] + jnp.einsum(
                "hqk,khd->hqd",
                raised.astype(jnp.bfloat16),
                values_here,
                preferred_element_type=jnp.float32,
            )
            return (top_new, totals, weighted)

        return (lax.cond(key_pos[0] <= last_query, advance, keep_state, state), None)

    running, _ = lax.scan(update, running, jnp.arange(amount // span_rows))
    return running


def mixer_half(query, latent, rope_key, latent_gain, key_up, value_up, out_proj):
    query_rows = query.shape[0]
    own_rows = latent.shape[0]
    query_start = lax.axis_index("ep") * query_rows
    key_start = query_start + lax.axis_index("tp") * own_rows
    head_count = query.shape[1] // (NOPE + ROPE_DIM)
    normed = rms_scale(latent, latent_gain).astype(jnp.bfloat16)
    key_cos, key_sin = tables(key_start + jnp.arange(own_rows, dtype=jnp.int32), ROPE_DIM)
    rotated_key = rotate(rope_key.astype(jnp.float32), key_cos, key_sin).astype(jnp.bfloat16)
    query_pos = query_start + jnp.arange(query_rows, dtype=jnp.int32)
    query_cos, query_sin = tables(query_pos, ROPE_DIM)
    query_heads = query.reshape(query_rows, head_count, NOPE + ROPE_DIM)
    turned = rotate(
        query_heads[..., NOPE:].astype(jnp.float32), query_cos[:, None, :], query_sin[:, None, :]
    ).astype(jnp.bfloat16)
    query_rot = jnp.concatenate([query_heads[..., :NOPE], turned], axis=-1)
    last_query = query_start + query_rows - 1
    initial = (
        jnp.full((head_count, query_rows), masked_value, jnp.float32),
        jnp.zeros((head_count, query_rows), jnp.float32),
        jnp.zeros((head_count, query_rows, V_DIM), jnp.float32),
    )
    shard_rows = (
        lax.all_gather(normed, ("ep", "tp"), axis=0, tiled=True),
        lax.all_gather(rotated_key, ("ep", "tp"), axis=0, tiled=True),
    )

    def compute(state_in):
        key_part = jnp.dot(shard_rows[0], key_up, preferred_element_type=jnp.float32).astype(
            jnp.bfloat16
        )
        value_part = jnp.dot(shard_rows[0], value_up, preferred_element_type=jnp.float32).astype(
            jnp.bfloat16
        )
        return attend_block(state_in, query_rot, query_pos, key_part, value_part, shard_rows[1])

    running = lax.cond(jnp.int32(0) <= last_query, compute, keep_state, initial)
    totals = running[1]
    weighted = running[2]
    attention = (
        (weighted / totals[..., None])
        .transpose(1, 0, 2)
        .reshape(query_rows, head_count * V_DIM)
        .astype(jnp.bfloat16)
    )
    own_attention = lax.all_to_all(attention, "tp", split_axis=0, concat_axis=1, tiled=True)
    return jnp.dot(own_attention, out_proj, preferred_element_type=jnp.float32).astype(jnp.bfloat16)


def expert_half(tokens, moe_gain, routes, group_prob, expert_prob, w_gate, w_up, w_down):
    row_count, model_width = tokens.shape
    top_count = routes.shape[1]
    expert_count = lax.axis_size("ep")
    capacity = 2 * top_count * row_count // expert_count
    normed = rms_scale(tokens, moe_gain).astype(jnp.bfloat16)
    flat_routes = routes.reshape(-1)
    onehot = (flat_routes[:, None] == jnp.arange(expert_count, dtype=jnp.int32)[None, :]).astype(
        jnp.int32
    )
    earlier = jnp.cumsum(onehot, axis=0) - onehot
    slot_index = jnp.sum(earlier * onehot, axis=1)
    target = flat_routes * capacity + slot_index
    owner = target[None, :] == jnp.arange(expert_count * capacity, dtype=jnp.int32)[:, None]
    dispatch_table = jnp.any(
        owner.reshape(expert_count * capacity, row_count, top_count), axis=2
    ).astype(jnp.bfloat16)
    outgoing = jnp.dot(dispatch_table, normed, preferred_element_type=jnp.float32).astype(
        jnp.bfloat16
    )
    outgoing = outgoing.reshape(expert_count, capacity, model_width)
    arrived = lax.all_to_all(outgoing, "ep", split_axis=0, concat_axis=0, tiled=True)
    sources, slots, _ = arrived.shape
    flat_rows = arrived.reshape(sources * slots, model_width)
    shard_rows = lax.all_gather(flat_rows, "tp", axis=0, tiled=True)
    gate_values = jnp.dot(shard_rows, w_gate[0], preferred_element_type=jnp.float32)
    up_values = jnp.dot(shard_rows, w_up[0], preferred_element_type=jnp.float32)
    hidden = (jax.nn.silu(gate_values) * up_values).astype(jnp.bfloat16)

    def lower(offset, amount):
        return jnp.dot(hidden, w_down[0], preferred_element_type=jnp.float32)

    summed = lax.psum_scatter(
        lower(jnp.int32(0), sources * slots * lax.axis_size("tp")).astype(jnp.bfloat16),
        "tp",
        scatter_dimension=0,
        tiled=True,
    )
    result = summed.reshape(sources, slots, model_width)
    returned = lax.all_to_all(result, "ep", split_axis=0, concat_axis=0, tiled=True)
    returned_flat = returned.reshape(expert_count * capacity, model_width)
    picked = returned_flat[target].reshape(row_count, top_count, model_width).astype(jnp.float32)
    shares = group_prob[:, None] * expert_prob / jnp.sum(expert_prob, axis=1, keepdims=True)
    return jnp.sum(shares[:, :, None] * picked, axis=1).astype(jnp.bfloat16)


def body(
    query,
    latent,
    rope_key,
    latent_gain,
    key_up,
    value_up,
    out_proj,
    tokens,
    moe_gain,
    routes,
    group_prob,
    expert_prob,
    w_gate,
    w_up,
    w_down,
):
    mixed = mixer_half(query, latent, rope_key, latent_gain, key_up, value_up, out_proj)
    moe_out = expert_half(tokens, moe_gain, routes, group_prob, expert_prob, w_gate, w_up, w_down)
    return (mixed, moe_out)


def solution(mesh):
    return jax.shard_map(
        body,
        mesh=mesh,
        in_specs=(
            P("ep", "tp"),
            P(("ep", "tp"), None),
            P(("ep", "tp"), None),
            P(),
            P(None, "tp"),
            P(None, "tp"),
            P(),
            P(("ep", "tp"), None),
            P(),
            P(("ep", "tp"), None),
            P(("ep", "tp")),
            P(("ep", "tp"), None),
            P("ep", None, "tp"),
            P("ep", None, "tp"),
            P("ep", "tp", None),
        ),
        out_specs=(P(("ep", "tp"), None), P(("ep", "tp"), None)),
        check_vma=False,
    )
```

profile of v0, /device:TPU:0, one launch (start us, length us, event | category | flops | bytes accessed | tf_op | source)
XLA Modules:
  0.0 223.9 jit_solution(14774280976944361633)
XLA Ops:
  7.2 0.8 copy.68
  8.8 0.6 broadcast_multiply_fusion
  9.6 1.1 fusion.27
  10.8 1.6 convolution_convert_fusion.3
  12.3 33.0 %all_to_all.26 = bf16[8,32,2048]{2,1,0:T(8,128)(2,1)} all-to-all(bf16[8,32,2048]{2,1,0:T(8,128)(2,1)S(1)} %bitcast.53), channel_id=1, replica_groups=mesh['ep'=8,'tp'=4] {'ep'}, dimensions={0} | all-to-all | bytes 2097152 | tf_op jit(solution)/shard_map/all_to_all | solution.py:156
  45.5 0.7 fusion.37
  46.3 32.6 %all-gather.5.cloned.1.call-done = bf16[1024,2048]{1,0:T(8,128)(2,1)} async-done(((bf16[256,2048]{1,0:T(8,128)(2,1)}), bf16[1024,2048]{1,0:T(8,128)(2,1)}) %all-gather.5.cloned.1.call-update) | async-done | bytes 4194320 | tf_op jit(solution)/shard_map/all_gather | solution.py:159
  78.9 4.4 %fusion.20 = f32[1024,256]{1,0:T(8,128)} fusion(bf16[1024,2048]{1,0:T(8,128)(2,1)} %all-gather.5.cloned.1.call-done, bf16[1,2048,256]{2,1,0:T(8,128)(2,1)S(1)} %copy-done.11), kind=kOutput, calls=%fused_computation.33 | convolution fusion | flops 1073741824 | bytes 6291456 | tf_op jit(solution)/shard_map/dot_general | solution.py:160
  83.3 8.8 %convolution_convert_fusion.2 = bf16[1024,2048]{1,0:T(8,128)(2,1)} fusion(bf16[1024,2048]{1,0:T(8,128)(2,1)} %all-gather.5.cloned.1.call-done, bf16[1,256,2048]{2,1,0:T(8,128)(2,1)S(1)} %copy-done, bf16[1,2048,256]{2,1,0:T(8,128)(2,1)S(1)} %copy-done.12, f32[1024,256]{1,0:T(8,128)} %fusion.20), kind=kOutput, calls=%fused_computation.26 | convolution fusion | flops 2151153664 | bytes 11534336 | tf_op jit(solution)/shard_map/dot_general | solution.py:165
  92.2 0.8 copy-done.6
  93.5 41.5 %all_gather.10 = bf16[1024,32]{1,0:T(8,128)(2,1)S(1)} all-gather(bf16[32,32]{1,0:T(8,128)(2,1)S(1)} %copy.62), channel_id=1, replica_groups=mesh['ep'=8,'tp'=4] {'ep','tp'}, dimensions={0}, use_global_device_ids=true | all-gather | bytes 67584 | tf_op jit(solution)/shard_map/all_gather | solution.py:110
  135.2 1.1 all-gather.3.cloned.1.call-done
  136.2 14.5 %conditional.2 = ((f32[4,128]{1,0:T(4,128)}, f32[4,128,64]{1,2,0:T(8,128)})) conditional(s32[]{:T(128)} %convert_element_type.90, () %tuple.32, (s32[]{:T(128)}, s32[128]{0:T(128)S(1)}, bf16[1024,512]{1,0:T(8,128)(2,1)}, bf16[512,256]{1,0:T(8,128)(2,1)S(1)}, bf16[512,256]{1,0:T(8,128)(2,1)S(1)}, /*index=5*/bf16[1024,32]{1,0:T(8,128)(2,1)S(1)}, ...), branch_computations={%region_1.0_spmd, %region_2.7_spmd} | conditional | flops 713754240 | bytes 23273134 | solution.py:122
  136.2 1.7 convolution_convert_fusion
  137.9 1.7 convolution_convert_fusion.1
  139.6 0.7 broadcast_in_dim.74
  140.8 0.6 slice.18
  141.4 0.6 slice.17
  143.2 7.5 %conditional = ((f32[4,128]{1,0:T(4,128)}, f32[4,128,64]{1,2,0:T(8,128)})) conditional(s32[]{:T(128)} %bitcast.3, (f32[4,128]{1,0:T(4,128)}, f32[4,128,64]{1,2,0:T(8,128)}) %tuple.26, (s32[1024]{0:T(1024)S(1)}, s32[128]{0:T(128)S(1)}, bf16[1024,256]{1,0:T(8,128)(2,1)S(1)}, bf16[1024,32]{1,0:T(8,128)(2,1)S(1)}, bf16[128,4,96]{0,2,1:T(8,128)(2,1)S(1)}, ...), branch_computations={%region_3.3_spmd, %region_4.6_spmd} | conditional | flops 176358912 | bytes 19460660 | solution.py:80
  143.8 0.6 fusion
  144.4 1.3 copy-done.1
  146.3 1.2 subtract_exponential_fusion
  147.7 3.1 %convolution_add_fusion = f32[4,128,64]{1,2,0:T(8,128)} fusion(bf16[1024,4,64]{0,2,1:T(8,128)(2,1)S(1)} %bitcast.56, f32[4,1024,128]{2,1,0:T(8,128)} %copy-done.1, f32[4,128]{1,0:T(4,128)S(1)} %broadcast_maximum_fusion, pred[128,1024]{0,1:T(8,128)(4,1)S(1)} %broadcast_compare_fusion, f32[4,128,64]{1,2,0:T(8,128)} %get-tuple-element.110, ...), kind=kOutput, calls=%fused_computation.6 | convolution fusion | flops 69795840 | bytes 3018752 | tf_op jit(solution)/shard_map/cond/branch_1_fun/while/body/eval_jaxpr/cond/branch_1_fun/hqk,khd->hqd/dot_general | solution.py:72
  150.7 1.0 fusion.39
  152.0 6.6 %all_to_all.27 = bf16[4,32,256]{2,1,0:T(8,128)(2,1)S(1)} all-to-all(bf16[4,32,256]{2,1,0:T(8,128)(2,1)S(1)} %convert_element_type.99), channel_id=1, replica_groups=mesh['ep'=8,'tp'=4] {'tp'}, dimensions={0} | all-to-all | bytes 131072 | tf_op jit(solution)/shard_map/all_to_all | solution.py:131
  158.6 23.9 %reduce-scatter.2.cloned.1.call-done = bf16[256,2048]{1,0:T(8,128)(2,1)} async-done(((bf16[1024,2048]{1,0:T(8,128)(2,1)}), bf16[256,2048]{1,0:T(8,128)(2,1)}) %reduce-scatter.2.cloned.1.call-update) | async-done | bytes 1048592 | tf_op jit(solution)/shard_map/reduce_scatter | solution.py:167
  182.5 5.4 %all-to-all-start.2 = ((bf16[8,32,2048]{2,1,0:T(8,128)(2,1)}), bf16[8,32,2048]{2,1,0:T(8,128)(2,1)S(1)}, u32[]{:S(2)}, u32[]{:S(2)}) async-start(bf16[8,32,2048]{2,1,0:T(8,128)(2,1)} %bitcast.54), calls=%async_computation.3 | async-start | bytes 2097152 | tf_op jit(solution)/shard_map/all_to_all | solution.py:174
  188.2 3.7 %convolution_convert_fusion.4 = bf16[32,2048]{1,0:T(8,128)(2,1)} fusion(bf16[32,1024]{1,0:T(8,128)(2,1)S(1)} %bitcast.59, bf16[1024,2048]{1,0:T(8,128)(2,1)} %param.25), kind=kOutput, calls=%fused_computation.28 | convolution fusion | flops 134283264 | bytes 4390912 | tf_op jit(solution)/shard_map/dot_general | solution.py:132
  191.9 21.7 %all-to-all-done.2 = bf16[8,32,2048]{2,1,0:T(8,128)(2,1)S(1)} async-done(((bf16[8,32,2048]{2,1,0:T(8,128)(2,1)}), bf16[8,32,2048]{2,1,0:T(8,128)(2,1)S(1)}, u32[]{:S(2)}, u32[]{:S(2)}) %all-to-all-start.2) | async-done | bytes 1048608 | tf_op jit(solution)/shard_map/all_to_all | solution.py:174
  213.6 0.9 gather_fusion
  214.5 0.7 reshape.210
  215.2 2.2 multiply_reduce_fusion
  (75 shorter events, 4.2 us)
Async XLA Ops:
  7.2 76.2 %copy-start = (bf16[1,256,2048]{2,1,0:T(8,128)(2,1)S(1)}, bf16[1,256,2048]{2,1,0:T(8,128)(2,1)}, u32[]{:S(2)}) copy-start(bf16[1,256,2048]{2,1,0:T(8,128)(2,1)} %param.33) | copy-start | bytes 3145732
  7.2 71.8 %all-gather.5.cloned.1.call-start = ((), (), s32[]{:S(2)}) async-start(), calls=%async_computation.5 | async-start | bytes 5242880 | tf_op jit(solution)/shard_map/all_gather | solution.py:159
  10.7 34.6 %copy-start.4 = (bf16[32,512]{1,0:T(8,128)(2,1)S(1)}, bf16[32,512]{1,0:T(8,128)(2,1)}, u32[]{:S(2)}) copy-start(bf16[32,512]{1,0:T(8,128)(2,1)} %param.20) | copy-start | bytes 98308
  10.7 34.8 %copy-start.9 = (f32[512]{0:T(512)S(1)}, f32[512]{0:T(512)}, u32[]{:S(2)}) copy-start(f32[512]{0:T(512)} %param.22) | copy-start | bytes 6148
  10.8 68.2 %copy-start.11 = (bf16[1,2048,256]{2,1,0:T(8,128)(2,1)S(1)}, bf16[1,2048,256]{2,1,0:T(8,128)(2,1)}, u32[]{:S(2)}) copy-start(bf16[1,2048,256]{2,1,0:T(8,128)(2,1)} %param.31) | copy-start | bytes 3145732
  45.3 90.9 %all-gather.3.cloned.1.call-start = ((), (), s32[]{:S(2)}) async-start(), calls=%async_computation.4 | async-start | bytes 1081344 | tf_op jit(solution)/shard_map/all_gather | solution.py:109
  46.2 37.1 %copy-start.12 = (bf16[1,2048,256]{2,1,0:T(8,128)(2,1)S(1)}, bf16[1,2048,256]{2,1,0:T(8,128)(2,1)}, u32[]{:S(2)}) copy-start(bf16[1,2048,256]{2,1,0:T(8,128)(2,1)} %param.32) | copy-start | bytes 3145732
  46.2 136.3 %reduce-scatter.2.cloned.1.call-start = ((), (), s32[]{:S(2)}) async-start(), calls=%async_computation.6 | async-start | bytes 5242880 | tf_op jit(solution)/shard_map/reduce_scatter | solution.py:167
  92.1 0.9 copy-start.6
  92.1 1.0 copy-start.7
  92.1 44.1 %copy-start.2 = (bf16[512,256]{1,0:T(8,128)(2,1)S(1)}, bf16[512,256]{1,0:T(8,128)(2,1)}, u32[]{:S(2)}) copy-start(bf16[512,256]{1,0:T(8,128)(2,1)} %param.23) | copy-start | bytes 786436
  92.1 44.1 %copy-start.3 = (bf16[512,256]{1,0:T(8,128)(2,1)S(1)}, bf16[512,256]{1,0:T(8,128)(2,1)}, u32[]{:S(2)}) copy-start(bf16[512,256]{1,0:T(8,128)(2,1)} %param.24) | copy-start | bytes 786436
  144.4 1.3 copy-start.1
  150.7 37.2 %copy-start.5 = (s32[64,2]{1,0:T(8,128)S(1)}, s32[64,2]{1,0:T(8,128)}, u32[]{:S(2)}) copy-start(s32[64,2]{1,0:T(8,128)} %get-tuple-element.197) | copy-start | bytes 1540
  150.7 37.3 %copy-start.8 = (f32[64,2]{0,1:T(2,128)S(1)}, f32[64,2]{0,1:T(2,128)}, u32[]{:S(2)}) copy-start(f32[64,2]{0,1:T(2,128)} %param.30) | copy-start | bytes 1540
  150.7 37.4 %copy-start.10 = (f32[64]{0:T(128)S(1)}, f32[64]{0:T(128)}, u32[]{:S(2)}) copy-start(f32[64]{0:T(128)} %param.29) | copy-start | bytes 772
  182.5 31.1 %all-to-all-start.2 = ((bf16[8,32,2048]{2,1,0:T(8,128)(2,1)}), bf16[8,32,2048]{2,1,0:T(8,128)(2,1)S(1)}, u32[]{:S(2)}, u32[]{:S(2)}) async-start(bf16[8,32,2048]{2,1,0:T(8,128)(2,1)} %bitcast.54), calls=%async_computation.3 | async-start | bytes 2097152 | tf_op jit(solution)/shard_map/all_to_all | solution.py:174
Sparse Core Ops, SparseCore 0:
  45.4 33.4 all-gather.4
  82.4 53.8 all-gather.2
  138.8 43.6 reduce-scatter.1
where the time goes:
time: 225 us; the launch traced here: 224 us
  blocking collectives  81.1 us (36%)
  waiting for transfers between devices  79.3 us (35%)
  matrix products  25.4 us (11%)
  between operations  14 us (6%)
  local copies, waits for them, and re-layouts  8.74 us (4%)
  other arithmetic  8.56 us (4%)
  starting transfers between devices  5.53 us (2%)
    all_gather x1, blocking collectives, mixer_half(): lax.all_gather(rotated_key, ('ep', 'tp'), axis=0, tiled=True)  41.5 us
    all_to_all x1, blocking collectives, expert_half(): lax.all_to_all(outgoing, 'ep', split_axis=0, concat_axis=0, tiled=True)  33 us
    all_gather x1, waiting for transfers between devices, expert_half(): shard_rows = lax.all_gather(flat_rows, 'tp', axis=0, tiled=True)  32.6 us
    reduce_scatter x1, waiting for transfers between devices, expert_half(): lax.psum_scatter(lower(jnp.int32(0), sources * slots * lax.axis_size('tp'...  23.9 us
    all_to_all x1, waiting for transfers between devices, expert_half(): lax.all_to_all(result, 'ep', split_axis=0, concat_axis=0, tiled=True)  21.7 us
    dot_general x1, matrix products, lower(): return jnp.dot(hidden, w_down[0], preferred_element_type=jnp.float32)  8.77 us
    all_to_all x1, blocking collectives, mixer_half(): lax.all_to_all(attention, 'tp', split_axis=0, concat_axis=1, tiled=True)  6.64 us
    all_to_all x1, starting transfers between devices, expert_half(): lax.all_to_all(result, 'ep', split_axis=0, concat_axis=0, tiled=True)  5.41 us
  transfers between devices with their start and end apart: 4, of which 4 were waited for; matrix products, arithmetic and copies ran while one was open for 14% of the time, Pallas kernels for 0%

commit v1 on v0

--- a/solution.py
+++ b/solution.py
@@ -156,7 +156,12 @@
     arrived = lax.all_to_all(outgoing, "ep", split_axis=0, concat_axis=0, tiled=True)
     sources, slots, _ = arrived.shape
     flat_rows = arrived.reshape(sources * slots, model_width)
-    shard_rows = lax.all_gather(flat_rows, "tp", axis=0, tiled=True)
+    ring = [flat_rows]
+    for hop in range(3):
+        ring.append(lax.ppermute(ring[-1], "tp", [(dev, (dev + 1) % 4) for dev in range(4)]))
+    shard_rows = jnp.roll(
+        jnp.concatenate(ring[::-1], axis=0), (lax.axis_index("tp") + 1) * ring[0].shape[0], axis=0
+    )
     gate_values = jnp.dot(shard_rows, w_gate[0], preferred_element_type=jnp.float32)
     up_values = jnp.dot(shard_rows, w_up[0], preferred_element_type=jnp.float32)
     hidden = (jax.nn.silu(gate_values) * up_values).astype(jnp.bfloat16)

time: 225 us -> 213 us (0.947)
  waiting for transfers between devices: 79.3 us -> 63.4 us
  local copies, waits for them, and re-layouts: 8.74 us -> 17.5 us
  matrix products: 25.4 us -> 21.8 us
    ppermute x0 -> x3, waiting for transfers between devices: none -> 42.4 us  [expert_half(): lax.ppermute(ring[-1], 'tp', [(dev, (dev + 1) % 4) for dev in range(4)])]
    all_gather x1 -> x0, waiting for transfers between devices: 32.6 us -> none  [expert_half(): shard_rows = lax.all_gather(flat_rows, 'tp', axis=0, tiled=True)]
    reduce_scatter x1, waiting for transfers between devices: 23.9 us -> 0.01 us  [expert_half(): lax.psum_scatter(lower(jnp.int32(0), sources * slots * lax.axis_size('tp'...]
    unnamed x27 -> x32, local copies, waits for them, and re-layouts: 1.96 us -> 10.6 us
    dot_general x1, matrix products: 4.39 us -> 1.25 us  [expert_half(): up_values = jnp.dot(shard_rows, w_up[0], preferred_element_type=jnp.float32)]
  transfers between devices with their start and end apart: 4 -> 6, of which waited for: 4 -> 4; matrix products, arithmetic and copies ran while one was open for 14% -> 16% of each run, Pallas kernels for 0% -> 0%
where the time goes in v1:
time: 213 us; the launch traced here: 212 us
  blocking collectives  80.1 us (38%)
  waiting for transfers between devices  63.4 us (30%)
  matrix products  21.8 us (10%)
  local copies, waits for them, and re-layouts  17.5 us (8%)
  between operations  15.9 us (7%)
  other arithmetic  8.64 us (4%)
  starting transfers between devices  3.83 us (2%)
    ppermute x3, waiting for transfers between devices, expert_half(): lax.ppermute(ring[-1], 'tp', [(dev, (dev + 1) % 4) for dev in range(4)])  42.4 us
    all_gather x1, blocking collectives, mixer_half(): lax.all_gather(rotated_key, ('ep', 'tp'), axis=0, tiled=True)  40.7 us
    all_to_all x1, blocking collectives, expert_half(): lax.all_to_all(outgoing, 'ep', split_axis=0, concat_axis=0, tiled=True)  32.9 us
    all_to_all x1, waiting for transfers between devices, expert_half(): lax.all_to_all(result, 'ep', split_axis=0, concat_axis=0, tiled=True)  21 us
    unnamed x32, local copies, waits for them, and re-layouts  10.6 us
    dot_general x1, matrix products, lower(): return jnp.dot(hidden, w_down[0], preferred_element_type=jnp.float32)  8.5 us
    all_to_all x1, blocking collectives, mixer_half(): lax.all_to_all(attention, 'tp', split_axis=0, concat_axis=1, tiled=True)  6.49 us
  transfers between devices with their start and end apart: 6, of which 4 were waited for; matrix products, arithmetic and copies ran while one was open for 16% of the time, Pallas kernels for 0%

profile of v1, /device:TPU:0, one launch (start us, length us, event | category | flops | bytes accessed | tf_op | source)
XLA Modules:
  0.0 212.5 jit_solution(13588335640509664730)
XLA Ops:
  8.1 0.8 copy.68
  9.8 1.1 fusion.23
  11.0 1.5 convolution_convert_fusion.3
  12.4 32.9 %all_to_all.26 = bf16[8,32,2048]{2,1,0:T(8,128)(2,1)S(1)} all-to-all(bf16[8,32,2048]{2,1,0:T(8,128)(2,1)S(1)} %bitcast.56), channel_id=1, replica_groups=mesh['ep'=8,'tp'=4] {'ep'}, dimensions={0} | all-to-all | bytes 2097152 | tf_op jit(solution)/shard_map/all_to_all | solution.py:156
  45.3 14.2 %collective-permute-done = bf16[256,2048]{1,0:T(8,128)(2,1)S(1)} collective-permute-done((bf16[256,2048]{1,0:T(8,128)(2,1)S(1)}, bf16[256,2048]{1,0:T(8,128)(2,1)S(1)}, u32[]{:S(2)}, u32[]{:S(2)}) %collective-permute-start) | collective-permute-done | bytes 1048608 | tf_op jit(solution)/shard_map/ppermute | solution.py:161
  59.5 14.3 %collective-permute-done.1 = bf16[256,2048]{1,0:T(8,128)(2,1)} collective-permute-done((bf16[256,2048]{1,0:T(8,128)(2,1)S(1)}, bf16[256,2048]{1,0:T(8,128)(2,1)}, u32[]{:S(2)}, u32[]{:S(2)}) %collective-permute-start.1) | collective-permute-done | bytes 1048608 | tf_op jit(solution)/shard_map/ppermute | solution.py:161
  74.0 0.7 fusion.41
  74.8 13.9 %collective-permute-done.2 = bf16[256,2048]{1,0:T(8,128)(2,1)} collective-permute-done((bf16[256,2048]{1,0:T(8,128)(2,1)}, bf16[256,2048]{1,0:T(8,128)(2,1)}, u32[]{:S(2)}, u32[]{:S(2)}) %collective-permute-start.2) | collective-permute-done | bytes 1048608 | tf_op jit(solution)/shard_map/ppermute | solution.py:161
  88.7 1.3 constant_dynamic-update-slice_fusion.7
  89.9 1.3 constant_dynamic-update-slice_fusion.6
  91.4 1.4 constant_dynamic-update-slice_fusion.3
  92.8 1.3 constant_dynamic-update-slice_fusion.2
  94.3 3.2 %copy-done.4 = bf16[2048,2048]{1,0:T(8,128)(2,1)} copy-done((bf16[2048,2048]{1,0:T(8,128)(2,1)}, bf16[2048,2048]{1,0:T(8,128)(2,1)S(1)}, u32[]{:S(2)}) %copy-start.4) | copy-done | bytes 8388632
  97.5 1.2 fusion.16
  98.8 8.5 %convolution_convert_fusion.2 = bf16[1024,2048]{1,0:T(8,128)(2,1)} fusion(bf16[1,256,2048]{2,1,0:T(8,128)(2,1)S(1)} %copy-done, f32[1024,256]{1,0:T(8,128)S(1)} %fusion.16, bf16[2048,2048]{1,0:T(8,128)(2,1)} %copy-done.4, s32[]{:T(128)S(6)} %select_n.39, bf16[1,2048,256]{2,1,0:T(8,128)(2,1)S(1)} %copy-done.11), kind=kOutput, calls=%fused_computation.26 | convolution fusion | flops 2151153664 | bytes 11534340 | tf_op jit(solution)/shard_map/dot_general | solution.py:170
  107.3 0.9 copy-done.6
  108.7 40.7 %all_gather.7 = bf16[1024,32]{1,0:T(8,128)(2,1)S(1)} all-gather(bf16[32,32]{1,0:T(8,128)(2,1)S(1)} %copy.62), channel_id=1, replica_groups=mesh['ep'=8,'tp'=4] {'ep','tp'}, dimensions={0}, use_global_device_ids=true | all-gather | bytes 67584 | tf_op jit(solution)/shard_map/all_gather | solution.py:110
  149.6 14.5 %conditional.2 = ((f32[4,128]{1,0:T(4,128)}, f32[4,128,64]{1,2,0:T(8,128)})) conditional(s32[]{:T(128)} %convert_element_type.90, () %tuple.32, (s32[]{:T(128)}, s32[128]{0:T(128)S(1)}, bf16[1024,512]{1,0:T(8,128)(2,1)}, bf16[512,256]{1,0:T(8,128)(2,1)S(1)}, bf16[512,256]{1,0:T(8,128)(2,1)S(1)}, /*index=5*/bf16[1024,32]{1,0:T(8,128)(2,1)S(1)}, ...), branch_computations={%region_1.0_spmd, %region_2.7_spmd} | conditional | flops 713754240 | bytes 23273134 | solution.py:122
  149.6 1.7 convolution_convert_fusion
  151.3 1.7 convolution_convert_fusion.1
  153.0 0.7 broadcast_in_dim.74
  156.6 7.5 %conditional = ((f32[4,128]{1,0:T(4,128)}, f32[4,128,64]{1,2,0:T(8,128)})) conditional(s32[]{:T(128)} %bitcast.3, (f32[4,128]{1,0:T(4,128)}, f32[4,128,64]{1,2,0:T(8,128)}) %tuple.26, (s32[1024]{0:T(1024)S(1)}, s32[128]{0:T(128)S(1)}, bf16[1024,256]{1,0:T(8,128)(2,1)S(1)}, bf16[1024,32]{1,0:T(8,128)(2,1)S(1)}, bf16[128,4,96]{0,2,1:T(8,128)(2,1)S(1)}, ...), branch_computations={%region_3.3_spmd, %region_4.6_spmd} | conditional | flops 176358912 | bytes 19460660 | solution.py:80
  157.9 1.3 copy-done.1
  159.7 1.3 subtract_exponential_fusion
  161.2 2.9 %convolution_add_fusion = f32[4,128,64]{1,2,0:T(8,128)} fusion(bf16[1024,4,64]{0,2,1:T(8,128)(2,1)S(1)} %bitcast.59, f32[4,1024,128]{2,1,0:T(8,128)} %copy-done.1, f32[4,128]{1,0:T(4,128)S(1)} %broadcast_maximum_fusion, pred[128,1024]{0,1:T(8,128)(4,1)S(1)} %broadcast_compare_fusion, f32[4,128,64]{1,2,0:T(8,128)} %get-tuple-element.110, ...), kind=kOutput, calls=%fused_computation.6 | convolution fusion | flops 69795840 | bytes 3018752 | tf_op jit(solution)/shard_map/cond/branch_1_fun/while/body/eval_jaxpr/cond/branch_1_fun/hqk,khd->hqd/dot_general | solution.py:72
  164.1 0.9 fusion.43
  165.4 6.5 %all_to_all.27 = bf16[4,32,256]{2,1,0:T(8,128)(2,1)S(1)} all-to-all(bf16[4,32,256]{2,1,0:T(8,128)(2,1)S(1)} %convert_element_type.99), channel_id=1, replica_groups=mesh['ep'=8,'tp'=4] {'tp'}, dimensions={0} | all-to-all | bytes 131072 | tf_op jit(solution)/shard_map/all_to_all | solution.py:131
  171.8 3.7 %all-to-all-start.2 = ((bf16[8,32,2048]{2,1,0:T(8,128)(2,1)}), bf16[8,32,2048]{2,1,0:T(8,128)(2,1)S(1)}, u32[]{:S(2)}, u32[]{:S(2)}) async-start(bf16[8,32,2048]{2,1,0:T(8,128)(2,1)} %bitcast.57), calls=%async_computation.3 | async-start | bytes 2097152 | tf_op jit(solution)/shard_map/all_to_all | solution.py:179
  176.6 3.7 %convolution_convert_fusion.4 = bf16[32,2048]{1,0:T(8,128)(2,1)} fusion(bf16[32,1024]{1,0:T(8,128)(2,1)S(1)} %bitcast.62, bf16[1024,2048]{1,0:T(8,128)(2,1)} %param.25), kind=kOutput, calls=%fused_computation.32 | convolution fusion | flops 134283264 | bytes 4390912 | tf_op jit(solution)/shard_map/dot_general | solution.py:132
  180.2 21.0 %all-to-all-done.2 = bf16[8,32,2048]{2,1,0:T(8,128)(2,1)S(1)} async-done(((bf16[8,32,2048]{2,1,0:T(8,128)(2,1)}), bf16[8,32,2048]{2,1,0:T(8,128)(2,1)S(1)}, u32[]{:S(2)}, u32[]{:S(2)}) %all-to-all-start.2) | async-done | bytes 1048608 | tf_op jit(solution)/shard_map/all_to_all | solution.py:179
  201.2 0.9 gather_fusion
  202.8 2.2 %multiply_reduce_fusion = bf16[64,2048]{1,0:T(8,128)(2,1)} fusion(f32[64,2,2048]{2,1,0:T(2,128)S(1)} %reshape.210, f32[64,2]{1,0:T(8,128)S(1)} %copy.67), kind=kLoop, calls=%fused_computation.36 | loop fusion | flops 393216 | bytes 1311232 | tf_op jit(solution)/shard_map/reduce_sum | solution.py:183
  (84 shorter events, 7.6 us)
Async XLA Ops:
  8.0 90.7 %copy-start = (bf16[1,256,2048]{2,1,0:T(8,128)(2,1)S(1)}, bf16[1,256,2048]{2,1,0:T(8,128)(2,1)}, u32[]{:S(2)}) copy-start(bf16[1,256,2048]{2,1,0:T(8,128)(2,1)} %param.33) | copy-start | bytes 3145732
  8.0 65.9 %copy-start.5 = (bf16[32,512]{1,0:T(8,128)(2,1)S(1)}, bf16[32,512]{1,0:T(8,128)(2,1)}, u32[]{:S(2)}) copy-start(bf16[32,512]{1,0:T(8,128)(2,1)} %param.20) | copy-start | bytes 98308
  8.0 66.0 %copy-start.9 = (f32[512]{0:T(512)S(1)}, f32[512]{0:T(512)}, u32[]{:S(2)}) copy-start(f32[512]{0:T(512)} %param.22) | copy-start | bytes 6148
  8.0 141.5 %all-gather.2.cloned.1.call-start = ((), (), s32[]{:S(2)}) async-start(), calls=%async_computation.4 | async-start | bytes 1081344 | tf_op jit(solution)/shard_map/all_gather | solution.py:109
  45.3 14.2 %collective-permute-start = (bf16[256,2048]{1,0:T(8,128)(2,1)S(1)}, bf16[256,2048]{1,0:T(8,128)(2,1)S(1)}, u32[]{:S(2)}, u32[]{:S(2)}) collective-permute-start(bf16[256,2048]{1,0:T(8,128)(2,1)S(1)} %bitcast.53), channel_id=1, source_target_pairs={{0,1},{1,2},{2,3},{3,0},{4,5},{5,6},{6,7},{7,4},{8,9},{9,10},{10,1... | collective-permute-start | bytes 3145736 | tf_op jit(solution)/shard_map/ppermute | solution.py:161
  59.5 14.3 %collective-permute-start.1 = (bf16[256,2048]{1,0:T(8,128)(2,1)S(1)}, bf16[256,2048]{1,0:T(8,128)(2,1)}, u32[]{:S(2)}, u32[]{:S(2)}) collective-permute-start(bf16[256,2048]{1,0:T(8,128)(2,1)S(1)} %collective-permute-done), channel_id=1, source_target_pairs={{0,1},{1,2},{2,3},{3,0},{4,5},{5,6},{6,7},{7,4},{8,9},{9,10},{10,1... | collective-permute-start | bytes 3145736 | tf_op jit(solution)/shard_map/ppermute | solution.py:161
  73.9 14.8 %collective-permute-start.2 = (bf16[256,2048]{1,0:T(8,128)(2,1)}, bf16[256,2048]{1,0:T(8,128)(2,1)}, u32[]{:S(2)}, u32[]{:S(2)}) collective-permute-start(bf16[256,2048]{1,0:T(8,128)(2,1)} %collective-permute-done.1), channel_id=1, source_target_pairs={{0,1},{1,2},{2,3},{3,0},{4,5},{5,6},{6,7},{7,4},{8,9},{9,10},{10,1... | collective-permute-start | bytes 3145736 | tf_op jit(solution)/shard_map/ppermute | solution.py:161
  74.7 97.1 %reduce-scatter.2.cloned.1.call-start = ((), (), s32[]{:S(2)}) async-start(), calls=%async_computation.5 | async-start | bytes 5242880 | tf_op jit(solution)/shard_map/reduce_scatter | solution.py:172
  91.4 6.1 %copy-start.10 = (bf16[1,2048,256]{2,1,0:T(8,128)(2,1)S(1)}, bf16[1,2048,256]{2,1,0:T(8,128)(2,1)}, u32[]{:S(2)}) copy-start(bf16[1,2048,256]{2,1,0:T(8,128)(2,1)} %param.32) | copy-start | bytes 3145732
  94.3 3.2 %copy-start.4 = (bf16[2048,2048]{1,0:T(8,128)(2,1)}, bf16[2048,2048]{1,0:T(8,128)(2,1)S(1)}, u32[]{:S(2)}) copy-start(bf16[2048,2048]{1,0:T(8,128)(2,1)S(1)} %constant_dynamic-update-slice_fusion) | copy-start | bytes 25165828
  97.5 1.3 copy-start.11
  107.3 0.9 copy-start.6
  107.3 1.0 copy-start.7
  107.3 42.3 %copy-start.2 = (bf16[512,256]{1,0:T(8,128)(2,1)S(1)}, bf16[512,256]{1,0:T(8,128)(2,1)}, u32[]{:S(2)}) copy-start(bf16[512,256]{1,0:T(8,128)(2,1)} %param.23) | copy-start | bytes 786436
  107.3 42.3 %copy-start.3 = (bf16[512,256]{1,0:T(8,128)(2,1)S(1)}, bf16[512,256]{1,0:T(8,128)(2,1)}, u32[]{:S(2)}) copy-start(bf16[512,256]{1,0:T(8,128)(2,1)} %param.24) | copy-start | bytes 786436
  149.6 26.1 %copy-start.8 = (f32[64,2]{0,1:T(2,128)S(1)}, f32[64,2]{0,1:T(2,128)}, u32[]{:S(2)}) copy-start(f32[64,2]{0,1:T(2,128)} %param.30) | copy-start | bytes 1540
  157.8 1.3 copy-start.1
  171.8 29.3 %all-to-all-start.2 = ((bf16[8,32,2048]{2,1,0:T(8,128)(2,1)}), bf16[8,32,2048]{2,1,0:T(8,128)(2,1)S(1)}, u32[]{:S(2)}, u32[]{:S(2)}) async-start(bf16[8,32,2048]{2,1,0:T(8,128)(2,1)} %bitcast.57), calls=%async_computation.3 | async-start | bytes 2097152 | tf_op jit(solution)/shard_map/all_to_all | solution.py:179
Sparse Core Ops, SparseCore 0:
  74.9 52.9 all-gather.1
Sparse Core Ops, SparseCore 1:
  107.4 44.6 reduce-scatter.1
